TPU v7x, 32 devices: a whole 2x2x4 slice. The times are simulated.
32 devices in a mesh: ep: 8 (over z, x), tp: 4 (over y, core).
Axes of the slice: x: 2, y: 2, z: 4, core: 2. Of those that a mesh axis runs over, the one named last changes fastest.
Arguments:
- hidden: bfloat16 [32, 2048], P('ep'), may hold values from -6 to 6
- attn_gain: float32 [2048], replicated, may hold values from 0.3 to 3
- query_weight: bfloat16 [2048, 2048], P('ep', 'tp'), may hold values from -0.125 to 0.125
- head_bias: float32 [16], replicated, may hold values from -10 to -4
- key_cache: bfloat16 [32, 4, 1024, 128], P('ep', 'tp'), may hold values from -6 to 6
- value_cache: bfloat16 [32, 4, 1024, 128], P('ep', 'tp'), may hold values from -7 to 7
- lengths: int32 [32], P('ep'), may hold values from 256 to 1024, as said below
- out_weight: bfloat16 [2048, 2048], P('tp', 'ep'), may hold values from -0.125 to 0.125
- moe_gain: float32 [2048], replicated, may hold values from 0.1 to 1.9
- route_group: int32 [32], P('ep'), may hold values from 0 to 1, as said below
- route_inner: int32 [32, 2], P('ep'), may hold values from 0 to 3, as said below
- route_weight: bfloat16 [32, 2], P('ep'), may hold values from 0.25 to 1
- gate_w: bfloat16 [8, 2048, 768], P('ep', None, 'tp'), may hold values from -0.125 to 0.125
- up_w: bfloat16 [8, 2048, 768], P('ep', None, 'tp'), may hold values from -0.125 to 0.125
- down_w: bfloat16 [8, 768, 2048], P('ep', 'tp'), may hold values from -0.21875 to 0.21875
Outputs:
- mixed: bfloat16 [32, 2048], P('ep', 'tp')
Inputs may be any that keep to these rules, and one draw needn't show every extreme that they name: `lengths`: some sequence has length 1024 in every draw. Within the rows of one device (aligned blocks of 4 rows) no expert route_group * 4 + route_inner is named twice; one expert is named in every block. `route_inner`: the 2 entries of a row differ.
All inputs are finite; a program needn't handle non-finite values.
Results may differ from a plain program's by a relative error of at most 0.013.
Values may be sent and summed in bfloat16 or wider, within the bound.
A program may use at most 64 MiB of HBM per device.

v0:
```python
import jax
import jax.numpy as jnp
from jax import lax
from jax.sharding import PartitionSpec as P

rms_epsilon = 1e-06


def rms_scale(values, gain):
    wide = values.astype(jnp.float32)
    scaled = wide * lax.rsqrt(jnp.mean(wide * wide, axis=-1, keepdims=True) + rms_epsilon)
    return (scaled * gain).astype(jnp.bfloat16)


def body(
    hidden,
    attn_gain,
    query_weight,
    head_bias,
    key_cache,
    value_cache,
    lengths,
    out_weight,
    moe_gain,
    route_group,
    route_inner,
    route_weight,
    gate_w,
    up_w,
    down_w,
):
    n_tp = lax.axis_size("tp")
    n_ep = lax.axis_size("ep")
    tokens = hidden.shape[0]
    d_model = hidden.shape[1]
    normed = rms_scale(hidden, attn_gain)
    feature_block = lax.all_to_all(normed, "ep", split_axis=1, concat_axis=0, tiled=True)
    queries = lax.psum_scatter(
        jnp.dot(feature_block, query_weight, preferred_element_type=jnp.float32),
        "ep",
        scatter_dimension=0,
        tiled=True,
    ).astype(jnp.bfloat16)
    head_size = key_cache.shape[3]
    local_kv = key_cache.shape[1]
    cache_len = key_cache.shape[2]
    local_heads = queries.shape[1] // head_size
    group_heads = local_heads // local_kv
    queries = queries.reshape(tokens, local_kv, group_heads, head_size)
    own_bias = lax.dynamic_slice_in_dim(
        head_bias, lax.axis_index("tp") * local_heads, local_heads, 0
    )
    own_bias = own_bias.reshape(local_kv, group_heads)
    scores = jnp.einsum(
        "tkgd,tkpd->tkgp", queries, key_cache, preferred_element_type=jnp.float32
    ) * head_size ** (-0.5)
    scores = scores + own_bias[None, :, :, None]
    position = jnp.arange(cache_len, dtype=jnp.int32)
    visible = position[None, None, None, :] < lengths[:, None, None, None]
    log_keep = jnp.where(visible, jax.nn.log_sigmoid(-scores), 0.0)
    later_sum = lax.cumsum(log_keep, axis=3, reverse=True) - log_keep
    weight = jnp.where(visible, jnp.exp(jax.nn.log_sigmoid(scores) + later_sum), 0.0).astype(
        jnp.bfloat16
    )
    heads_out = jnp.einsum(
        "tkgp,tkpd->tkgd", weight, value_cache, preferred_element_type=jnp.float32
    )
    heads_out = heads_out.astype(jnp.bfloat16).reshape(tokens, -1)
    partial_value = jnp.dot(
        heads_out,
        lax.all_gather(out_weight, "ep", axis=1, tiled=True),
        preferred_element_type=jnp.float32,
    )
    rounded = lax.optimization_barrier(partial_value.astype(jnp.bfloat16)).astype(jnp.float32)
    attended = lax.psum(rounded.astype(jnp.bfloat16), "tp").astype(jnp.float32)
    residual = (hidden.astype(jnp.float32) + attended).astype(jnp.bfloat16)
    normed_two = rms_scale(residual, moe_gain)
    per_device = gate_w.shape[0]
    experts = per_device * n_ep
    group_count = max(2, experts // 32)
    group_size = experts // group_count
    chosen = route_group[:, None] * group_size + route_inner
    matches = chosen[:, :, None] == jnp.arange(experts, dtype=jnp.int32)[None, None, :]
    picked = jnp.any(matches, axis=1).astype(jnp.bfloat16)
    mixing = jnp.sum(
        jnp.where(matches, route_weight[:, :, None].astype(jnp.float32), 0.0), axis=1
    ).astype(jnp.bfloat16)
    part_width = d_model // n_tp
    outgoing = jnp.einsum("te,td->ed", picked, normed_two, preferred_element_type=jnp.float32)
    outgoing = outgoing.astype(jnp.bfloat16).reshape(n_ep, per_device, d_model)
    arrived = lax.all_to_all(outgoing, "ep", split_axis=0, concat_axis=0, tiled=True)
    gated_in = jnp.einsum("sed,edf->sef", arrived, gate_w, preferred_element_type=jnp.float32)
    up_proj = jnp.einsum("sed,edf->sef", arrived, up_w, preferred_element_type=jnp.float32)
    activated = (jax.nn.silu(gated_in) * up_proj).astype(jnp.bfloat16)
    down_out = jnp.einsum("sef,efd->sed", activated, down_w, preferred_element_type=jnp.float32)
    down_rounded = lax.optimization_barrier(down_out.astype(jnp.bfloat16)).astype(jnp.float32)
    summed = lax.psum_scatter(
        down_rounded.astype(jnp.bfloat16), "tp", scatter_dimension=2, tiled=True
    )
    returned = lax.all_to_all(summed, "ep", split_axis=0, concat_axis=0, tiled=True).reshape(
        experts, part_width
    )
    routed = jnp.dot(mixing, returned, preferred_element_type=jnp.float32)
    own_residual = lax.dynamic_slice_in_dim(
        residual, lax.axis_index("tp") * part_width, part_width, 1
    )
    return (own_residual.astype(jnp.float32) + routed).astype(jnp.bfloat16)


def solution(mesh):
    placed = (
        P("ep", None),
        P(),
        P("ep", "tp"),
        P(),
        P("ep", "tp", None, None),
        P("ep", "tp", None, None),
        P("ep"),
        P("tp", "ep"),
        P(),
        P("ep"),
        P("ep", None),
        P("ep", None),
        P("ep", None, "tp"),
        P("ep", None, "tp"),
        P("ep", "tp", None),
    )
    return jax.shard_map(body, mesh=mesh, in_specs=placed, out_specs=P("ep", "tp"), check_vma=False)
```

profile of v0, /device:TPU:0, one launch (start us, length us, event | category | flops | bytes accessed | tf_op | source)
XLA Modules:
  0.0 150.5 jit_solution(8893848438040312585)
XLA Ops:
  6.5 0.7 all-gather.2.cloned.1.call-update
  7.3 0.8 fusion.25
  8.1 1.4 fusion.27
  9.5 7.3 %all-to-all-start = ((bf16[4,8,256]{2,0,1:T(4,128)(2,1)}), bf16[4,8,256]{2,0,1:T(4,128)(2,1)S(1)}, u32[]{:S(2)}, u32[]{:S(2)}) async-start(bf16[4,8,256]{2,0,1:T(4,128)(2,1)} %bitcast), calls=%async_computation | async-start | bytes 32768 | tf_op jit(solution)/shard_map/all_to_all | solution.py:37
  17.5 0.7 broadcast_add_fusion
  18.2 0.7 iota_compare_fusion
  19.5 0.7 dynamic_slice.6
  20.2 1.3 dynamic-slice
  22.1 1.4 all-to-all-done
  23.5 1.1 fusion.57
  24.6 37.7 %all-reduce = bf16[32,512]{1,0:T(8,128)(2,1)S(1)} all-reduce(f32[32,512]{1,0:T(8,128)S(1)} %fusion.57), channel_id=2, replica_groups=mesh['ep'=8,'tp'=4] {'ep'}, use_global_device_ids=true, to_apply=%region_1.0.clone | all-reduce | flops 16384 | bytes 98304
  62.8 19.8 %reduce-window.6 = f32[4,1,4,8,128]{4,3,2,1,0:T(8,128)S(1)} reduce-window(f32[4,1,4,8,128]{4,3,2,1,0:T(8,128)S(1)} %bitcast.82, f32[]{:T(128)} %constant.12.clone.1), window={size=1x1x1x1x128 pad=0_0x0_0x0_0x0_0x0_127}, to_apply=%region_2.3 | reduce-window | flops 2080768 | bytes 131076 | tf_op jit(solution)/shard_map/reduce-window
  82.7 0.7 reduce-window.9
  84.3 2.4 %fusion.6 = bf16[1,4,4,128]{3,2,1,0:T(4,128)(2,1)} fusion(bf16[4,1,1024,128]{3,2,1,0:T(8,128)(2,1)} %param.20, f32[4,4,1024]{2,1,0:T(4,128)S(1)} %reshape.148, f32[4,4,1024]{2,1,0:T(4,128)} %reshape.151, f32[4,4,1024]{2,1,0:T(4,128)S(1)} %get-tuple-element.8, pred[4,1024]{1,0:T(4,128)(4,1)} %copy-done.5), kind=kOutput, calls=%fused_computation.14 | convolution fusion | flops 4540416 | bytes 1253376 | tf_op jit(solution)/shard_map/tkgp,tkpd->tkgd/dot_general | solution.py:65
  86.6 2.0 %convolution_convert_fusion.2 = bf16[4,2048]{1,0:T(4,128)(2,1)S(1)} fusion(bf16[512,2048]{1,0:T(8,128)(2,1)} %all-gather.2.cloned.1.call-done, bf16[1,4,4,128]{3,2,1,0:T(4,128)(2,1)} %fusion.6), kind=kOutput, calls=%fused_computation.4 | convolution fusion | flops 8396800 | bytes 2117632 | tf_op jit(solution)/shard_map/dot_general | solution.py:69
  88.6 10.1 %psum.7 = bf16[4,2048]{1,0:T(4,128)(2,1)S(1)} all-reduce(bf16[4,2048]{1,0:T(4,128)(2,1)S(1)} %convolution_convert_fusion.2), channel_id=1, replica_groups=mesh['ep'=8,'tp'=4] {'tp'}, use_global_device_ids=true, to_apply=%region_4.5 | all-reduce | flops 8192 | bytes 32768 | tf_op jit(solution)/shard_map/psum | solution.py:75
  98.9 0.9 fusion
  101.0 9.1 %all_to_all.29 = bf16[8,2,1024]{2,1,0:T(2,128)(2,1)S(1)} all-to-all(bf16[8,2,1024]{2,1,0:T(2,128)(2,1)S(1)} %reshape.163), channel_id=1, replica_groups=mesh['ep'=8,'tp'=4] {'ep'}, dimensions={0} | all-to-all | bytes 65536 | tf_op jit(solution)/shard_map/all_to_all | solution.py:91
  110.4 1.3 fusion.1
  111.8 17.1 %reduce-scatter.2.cloned.1.call-done = bf16[8,1,512]{2,0,1:T(8,128)(2,1)} async-done(((bf16[8,1,2048]{2,0,1:T(8,128)(2,1)}), bf16[8,1,512]{2,0,1:T(8,128)(2,1)}) %reduce-scatter.2.cloned.1.call-update) | async-done | bytes 8208 | tf_op jit(solution)/shard_map/reduce_scatter | solution.py:97
  128.9 1.3 reduce.3
  130.9 5.5 %all-to-all-start.2 = ((bf16[8,2,256]{2,1,0:T(2,128)(2,1)}), bf16[8,2,256]{2,1,0:T(2,128)(2,1)S(1)}, u32[]{:S(2)}, u32[]{:S(2)}) async-start(bf16[8,2,256]{2,1,0:T(2,128)(2,1)} %reshape.165), calls=%async_computation.3 | async-start | bytes 16384 | tf_op jit(solution)/shard_map/all_to_all | solution.py:100
  136.5 6.4 %all-to-all-done.2 = bf16[8,2,256]{2,1,0:T(2,128)(2,1)S(1)} async-done(((bf16[8,2,256]{2,1,0:T(2,128)(2,1)}), bf16[8,2,256]{2,1,0:T(2,128)(2,1)S(1)}, u32[]{:S(2)}, u32[]{:S(2)}) %all-to-all-start.2) | async-done | bytes 8224 | tf_op jit(solution)/shard_map/all_to_all | solution.py:100
  142.9 0.7 fusion.4
  (46 shorter events, 5.1 us)
Async XLA Ops:
  6.5 55.8 %copy-start = (bf16[4,1,1024,128]{3,2,1,0:T(8,128)(2,1)S(1)}, bf16[4,1,1024,128]{3,2,1,0:T(8,128)(2,1)}, u32[]{:S(2)}) copy-start(bf16[4,1,1024,128]{3,2,1,0:T(8,128)(2,1)} %param.19) | copy-start | bytes 3145732
  6.5 80.1 %all-gather.2.cloned.1.call-start = ((), (), s32[]{:S(2)}) async-start(), calls=%async_computation.4 | async-start | bytes 2359296 | tf_op jit(solution)/shard_map/all_gather | solution.py:71
  9.5 14.0 %all-to-all-start = ((bf16[4,8,256]{2,0,1:T(4,128)(2,1)}), bf16[4,8,256]{2,0,1:T(4,128)(2,1)S(1)}, u32[]{:S(2)}, u32[]{:S(2)}) async-start(bf16[4,8,256]{2,0,1:T(4,128)(2,1)} %bitcast), calls=%async_computation | async-start | bytes 32768 | tf_op jit(solution)/shard_map/all_to_all | solution.py:37
  16.8 112.1 %reduce-scatter.2.cloned.1.call-start = ((), (), s32[]{:S(2)}) async-start(), calls=%async_computation.5 | async-start | bytes 40960 | tf_op jit(solution)/shard_map/reduce_scatter | solution.py:97
  18.2 5.3 %copy-start.6 = (s32[4,2]{0,1:T(2,128)}, s32[4,2]{0,1:T(2,128)S(1)}, u32[]{:S(2)}) copy-start(s32[4,2]{0,1:T(2,128)S(1)} %broadcast_add_fusion) | copy-start | bytes 100
  18.9 43.8 %copy-start.5 = (pred[4,1024]{1,0:T(4,128)(4,1)}, pred[4,1024]{1,0:T(4,128)(4,1)S(1)}, u32[]{:S(2)}) copy-start(pred[4,1024]{1,0:T(4,128)(4,1)S(1)} %iota_compare_fusion) | copy-start | bytes 12292
  62.8 36.0 %copy-start.4 = (bf16[4,2048]{1,0:T(4,128)(2,1)S(1)}, bf16[4,2048]{1,0:T(4,128)(2,1)}, u32[]{:S(2)}) copy-start(bf16[4,2048]{1,0:T(4,128)(2,1)} %param.15) | copy-start | bytes 49156
  83.5 26.6 %copy-start.1 = (bf16[1,2048,192]{1,2,0:T(8,128)(2,1)S(1)}, bf16[1,2048,192]{1,2,0:T(8,128)(2,1)}, u32[]{:S(2)}) copy-start(bf16[1,2048,192]{1,2,0:T(8,128)(2,1)} %param.27) | copy-start | bytes 2359300
  84.3 26.2 %copy-start.2 = (bf16[1,192,2048]{2,1,0:T(8,128)(2,1)S(1)}, bf16[1,192,2048]{2,1,0:T(8,128)(2,1)}, u32[]{:S(2)}) copy-start(bf16[1,192,2048]{2,1,0:T(8,128)(2,1)} %param.29) | copy-start | bytes 2359300
  84.3 26.2 %copy-start.3 = (bf16[1,2048,192]{1,2,0:T(8,128)(2,1)S(1)}, bf16[1,2048,192]{1,2,0:T(8,128)(2,1)}, u32[]{:S(2)}) copy-start(bf16[1,2048,192]{1,2,0:T(8,128)(2,1)} %param.28) | copy-start | bytes 2359300
  86.6 25.1 %copy-start.8 = (bf16[4,2]{0,1:T(2,128)(2,1)S(1)}, bf16[4,2]{0,1:T(2,128)(2,1)}, u32[]{:S(2)}) copy-start(bf16[4,2]{0,1:T(2,128)(2,1)} %param.26) | copy-start | bytes 52
  86.6 49.8 %copy-start.7 = (s32[4,2]{0,1:T(2,128)S(1)}, s32[4,2]{0,1:T(2,128)}, u32[]{:S(2)}) copy-start(s32[4,2]{0,1:T(2,128)} %copy-done.6) | copy-start | bytes 100
  130.9 12.0 %all-to-all-start.2 = ((bf16[8,2,256]{2,1,0:T(2,128)(2,1)}), bf16[8,2,256]{2,1,0:T(2,128)(2,1)S(1)}, u32[]{:S(2)}, u32[]{:S(2)}) async-start(bf16[8,2,256]{2,1,0:T(2,128)(2,1)} %reshape.165), calls=%async_computation.3 | async-start | bytes 16384 | tf_op jit(solution)/shard_map/all_to_all | solution.py:100
Sparse Core Ops, SparseCore 0:
  9.4 54.2 all-gather.1
  111.9 16.9 reduce-scatter.1
where the time goes:
time: 151 us; the launch traced here: 150 us
  blocking collectives  56.9 us (38%)
  other arithmetic  27.7 us (18%)
  waiting for transfers between devices  25.6 us (17%)
  between operations  14.1 us (9%)
  starting transfers between devices  12.8 us (8%)
  matrix products  9.09 us (6%)
  local copies, waits for them, and re-layouts  4.21 us (3%)
    unnamed x1, blocking collectives  37.7 us
    another operation x2, other arithmetic  20.5 us
    reduce_scatter x1, waiting for transfers between devices, body(): lax.psum_scatter(down_rounded.astype(jnp.bfloat16), 'tp', scatter_dimensi...  17.1 us
    psum x1, blocking collectives, body(): attended = lax.psum(rounded.astype(jnp.bfloat16), 'tp').astype(jnp.float32)  10.1 us
    all_to_all x1, blocking collectives, body(): lax.all_to_all(outgoing, 'ep', split_axis=0, concat_axis=0, tiled=True)  9.06 us
    all_to_all x1, starting transfers between devices, body(): lax.all_to_all(normed, 'ep', split_axis=1, concat_axis=0, tiled=True)  7.28 us
    all_to_all x1, waiting for transfers between devices, body(): lax.all_to_all(summed, 'ep', split_axis=0, concat_axis=0, tiled=True)  6.43 us
    all_to_all x1, starting transfers between devices, body(): lax.all_to_all(summed, 'ep', split_axis=0, concat_axis=0, tiled=True)  5.51 us
  transfers between devices with their start and end apart: 4, of which 3 were waited for; matrix products, arithmetic and copies ran while one was open for 22% of the time, Pallas kernels for 0%

commit v1 on v0

--- a/solution.py
+++ b/solution.py
@@ -1,6 +1,10 @@
+import functools
+
 import jax
 import jax.numpy as jnp
 from jax import lax
+from jax.experimental import pallas as pl
+from jax.experimental.pallas import tpu as pltpu
 from jax.sharding import PartitionSpec as P
 
 rms_epsilon = 1e-06
@@ -107,6 +111,512 @@
     return (own_residual.astype(jnp.float32) + routed).astype(jnp.bfloat16)
 
 
+MESH = pl.DeviceIdType.MESH
+
+
+def kernel(
+    n_ep,
+    n_tp,
+    group_size,
+    head_bias,
+    lengths,
+    route_group,
+    route_inner,
+    hidden_hbm,
+    attn_gain_hbm,
+    query_hbm,
+    key_hbm,
+    value_hbm,
+    out_hbm,
+    moe_gain_hbm,
+    route_weight_hbm,
+    gate_hbm,
+    up_hbm,
+    down_hbm,
+    mixed,
+    hidden,
+    attn_gain,
+    query_w,
+    keys,
+    values,
+    out_w,
+    moe_gain,
+    route_weight,
+    gate_w,
+    up_w,
+    down_w,
+    load_sem,
+    x_in,
+    r_out,
+    r_in,
+    q_out,
+    q_in,
+    h_out,
+    h_in,
+    a_out,
+    a_in,
+    m_out,
+    m_in,
+    z_out,
+    z_in,
+    x_send,
+    x_recv,
+    r_send,
+    r_recv,
+    q_send,
+    q_recv,
+    h_send,
+    h_recv,
+    a_send,
+    a_recv,
+    m_send,
+    m_recv,
+    z_send,
+    z_recv,
+    x_all,
+    route_all,
+    q_rows,
+    score_rows,
+    weight_rows,
+    head_rows,
+):
+    f32, bf16 = jnp.float32, jnp.bfloat16
+    ep = lax.axis_index("ep")
+    tp = lax.axis_index("tp")
+    tokens, d_model = hidden.shape
+    chunk = d_model // n_ep
+    total = tokens * n_ep
+    cache_len, head_size = keys.shape[1], keys.shape[2]
+    heads = query_w.shape[1] // head_size
+    rows = tokens * heads
+    part = d_model // n_tp
+    per_part = part // chunk
+    slots = route_inner.shape[1]
+
+    loads = [
+        pltpu.make_async_copy(src, dst, load_sem.at[index])
+        for index, (src, dst) in enumerate(
+            (
+                (hidden_hbm, hidden),
+                (attn_gain_hbm, attn_gain),
+                (query_hbm, query_w),
+                (key_hbm.at[:, 0], keys),
+                (value_hbm.at[:, 0], values),
+                (out_hbm, out_w),
+                (moe_gain_hbm, moe_gain),
+                (route_weight_hbm, route_weight),
+                (gate_hbm.at[0], gate_w),
+                (up_hbm.at[0], up_w),
+                (down_hbm.at[0], down_w),
+            )
+        )
+    ]
+    for load in loads:
+        load.start()
+
+    barrier = pltpu.get_barrier_semaphore()
+    others = [(i, j) for i in range(n_ep) for j in range(n_tp) if (i, j) != (0, 0)]
+    for i, j in others:
+        peer = (lax.rem(ep + i, n_ep), lax.rem(tp + j, n_tp))
+        pl.semaphore_signal(barrier, inc=1, device_id=peer, device_id_type=MESH)
+
+    lane = lax.broadcasted_iota(jnp.int32, (1, slots * 128), 1)
+    own_route = jnp.full((1, slots * 128), -1, jnp.int32)
+    chosen = [
+        [route_group[i] * group_size + route_inner[i, k] for k in range(slots)]
+        for i in range(tokens)
+    ]
+    for i in range(tokens):
+        for k in range(slots):
+            own_route = jnp.where(lane == k * 128 + ep * tokens + i, chosen[i][k], own_route)
+    r_out[...] = own_route
+
+    pl.semaphore_wait(barrier, len(others))
+    loads[0].wait()
+
+    sends = []
+
+    def push(src, dst, peer, send_sem, recv_sem):
+        copy = pltpu.make_async_remote_copy(
+            src_ref=src,
+            dst_ref=dst,
+            send_sem=send_sem,
+            recv_sem=recv_sem,
+            device_id=peer,
+            device_id_type=MESH,
+        )
+        copy.start()
+        sends.append(copy)
+
+    def arrived(ref, sem):
+        pltpu.make_async_copy(ref, ref, sem).wait()
+
+    def columns(index, width):
+        return pl.ds(pl.multiple_of(index * width, 128), width)
+
+    for k in range(1, n_ep):
+        to = lax.rem(ep + k, n_ep)
+        push(hidden.at[:, columns(to, chunk)], x_in.at[ep], (to, tp), x_send.at[k], x_recv.at[ep])
+    pltpu.make_async_copy(hidden.at[:, columns(ep, chunk)], x_in.at[ep], x_recv.at[ep]).start()
+    for k in range(1, n_ep):
+        to = lax.rem(ep + k, n_ep)
+        push(r_out, r_in.at[ep], (to, tp), r_send.at[k], r_recv.at[ep])
+    pltpu.make_async_copy(r_out, r_in.at[ep], r_recv.at[ep]).start()
+
+    wide = hidden[...].astype(f32)
+    scale = lax.rsqrt(jnp.mean(wide * wide, axis=-1, keepdims=True) + rms_epsilon)
+
+    loads[1].wait()
+    loads[2].wait()
+    for e in range(n_ep):
+        arrived(x_in.at[e], x_recv.at[e])
+        x_all[e * tokens : (e + 1) * tokens, :] = x_in[e].astype(f32)
+    features = (x_all[...] * attn_gain[:, columns(ep, chunk)]).astype(bf16)
+    query_parts = jnp.dot(features, query_w[...], preferred_element_type=f32)
+    for e in range(n_ep):
+        q_out[e] = query_parts[e * tokens : (e + 1) * tokens, :]
+    for k in range(1, n_ep):
+        to = lax.rem(ep + k, n_ep)
+        push(q_out.at[to], q_in.at[ep], (to, tp), q_send.at[k], q_recv.at[ep])
+    pltpu.make_async_copy(q_out.at[ep], q_in.at[ep], q_recv.at[ep]).start()
+
+    for e in range(n_ep):
+        arrived(r_in.at[e], r_recv.at[e])
+        for k in range(slots):
+            route_all[k, e : e + 1, :] = r_in[e, :, k * 128 : (k + 1) * 128]
+    tables = [route_all[k] for k in range(slots)]
+    picks = []
+    for e in range(n_ep):
+        hit = tables[0] == e
+        for table in tables[1:]:
+            hit = hit | (table == e)
+        picks.append(jnp.where(hit, 1.0, 0.0))
+    pick = jnp.concatenate(picks, axis=0)[:, :total].astype(bf16)
+
+    row = lax.broadcasted_iota(jnp.int32, (rows, 1), 0)
+    bias = jnp.zeros((rows, 1), f32)
+    length = jnp.zeros((rows, 1), jnp.int32)
+    for i in range(tokens):
+        length = jnp.where(row // heads == i, lengths[i], length)
+    for h in range(heads):
+        bias = jnp.where(row % heads == h, head_bias[tp * heads + h], bias)
+    above = lax.broadcasted_iota(jnp.int32, (128, 128), 0) > lax.broadcasted_iota(
+        jnp.int32, (128, 128), 1
+    )
+    above = jnp.where(above, 1.0, 0.0).astype(bf16)
+    loads[3].wait()
+
+    for e in range(n_ep):
+        arrived(q_in.at[e], q_recv.at[e])
+    queries = q_in[0]
+    for e in range(1, n_ep):
+        queries = queries + q_in[e]
+    queries = queries * scale
+    for i in range(tokens):
+        for h in range(heads):
+            q_rows[i * heads + h : i * heads + h + 1, :] = queries[
+                i : i + 1, h * head_size : (h + 1) * head_size
+            ]
+    for i in range(tokens):
+        score_rows[i * heads : (i + 1) * heads, :] = lax.dot_general(
+            q_rows[i * heads : (i + 1) * heads, :].astype(bf16),
+            keys[i],
+            (((1,), (1,)), ((), ())),
+            preferred_element_type=f32,
+        )
+    blocks = cache_len // 128
+    keeps, takes, seen = [], [], []
+    position = lax.broadcasted_iota(jnp.int32, (rows, 128), 1)
+    for c in range(blocks):
+        score = score_rows[:, c * 128 : (c + 1) * 128] * head_size ** (-0.5) + bias
+        visible = position + c * 128 < length
+        soft = jnp.log1p(jnp.exp(-jnp.abs(score)))
+        keeps.append(jnp.where(visible, -jnp.maximum(score, 0.0) - soft, 0.0))
+        takes.append(jnp.minimum(score, 0.0) - soft)
+        seen.append(visible)
+    keep = jnp.concatenate(keeps, axis=0)
+    high = keep.astype(bf16)
+    rest = keep - high.astype(f32)
+    middle = rest.astype(bf16)
+    low = (rest - middle.astype(f32)).astype(bf16)
+    later = (
+        jnp.dot(high, above, preferred_element_type=f32)
+        + jnp.dot(middle, above, preferred_element_type=f32)
+        + jnp.dot(low, above, preferred_element_type=f32)
+    )
+    tail = jnp.zeros((rows, 1), f32)
+    for c in reversed(range(blocks)):
+        exponent = takes[c] + later[c * rows : (c + 1) * rows, :] + tail
+        weight_rows[:, c * 128 : (c + 1) * 128] = jnp.where(seen[c], jnp.exp(exponent), 0.0)
+        tail = tail + jnp.sum(keeps[c], axis=1, keepdims=True)
+    loads[4].wait()
+    for i in range(tokens):
+        head_rows[i * heads : (i + 1) * heads, :] = jnp.dot(
+            weight_rows[i * heads : (i + 1) * heads, :].astype(bf16),
+            values[i],
+            preferred_element_type=f32,
+        )
+    h_out[...] = head_rows[:rows, :].astype(bf16)
+    for k in range(1, n_ep):
+        to = lax.rem(ep + k, n_ep)
+        push(h_out, h_in.at[ep], (to, tp), h_send.at[k], h_recv.at[ep])
+    pltpu.make_async_copy(h_out, h_in.at[ep], h_recv.at[ep]).start()
+
+    loads[5].wait()
+    for e in range(n_ep):
+        arrived(h_in.at[e], h_recv.at[e])
+        head_rows[e * rows : (e + 1) * rows, :] = h_in[e].astype(f32)
+    summed = x_all[...] * (1.0 / n_tp)
+    for h in range(heads):
+        summed = summed + jnp.dot(
+            head_rows[pl.ds(h, total, stride=heads), :].astype(bf16),
+            out_w[h * head_size : (h + 1) * head_size, :],
+            preferred_element_type=f32,
+        )
+    picked = jnp.dot(pick, summed.astype(bf16), preferred_element_type=f32)
+    for e in range(n_ep):
+        a_out[e] = picked[e * n_ep : (e + 1) * n_ep, :].astype(bf16)
+    for i, j in others:
+        to, side = lax.rem(ep + i, n_ep), lax.rem(tp + j, n_tp)
+        index = i * n_tp + j
+        push(a_out.at[to], a_in.at[ep, tp], (to, side), a_send.at[index], a_recv.at[ep, tp])
+    pltpu.make_async_copy(a_out.at[ep], a_in.at[ep, tp], a_recv.at[ep, tp]).start()
+
+    for e in range(n_ep):
+        m_out[e] = summed[e * tokens : (e + 1) * tokens, :].astype(bf16)
+    side, place = ep // per_part, lax.rem(ep, per_part)
+    for k in range(1, n_ep):
+        to = lax.rem(ep + k, n_ep)
+        push(m_out.at[to], m_in.at[place, tp], (to, side), m_send.at[k], m_recv.at[place, tp])
+
+    own = pltpu.make_async_remote_copy(
+        src_ref=m_out.at[ep],
+        dst_ref=m_in.at[place, tp],
+        send_sem=m_send.at[0],
+        recv_sem=m_recv.at[place, tp],
+        device_id=(ep, side),
+        device_id_type=MESH,
+    )
+
+    @pl.when(side != tp)
+    def _():
+        own.start()
+
+    @pl.when(side == tp)
+    def _():
+        pltpu.make_async_copy(m_out.at[ep], m_in.at[place, tp], m_recv.at[place, tp]).start()
+
+    for load in loads[6:]:
+        load.wait()
+    gated = jnp.zeros((n_ep, gate_w.shape[1]), f32)
+    upped = jnp.zeros((n_ep, up_w.shape[1]), f32)
+    squares = jnp.zeros((n_ep, 1), f32)
+    for e in range(n_ep):
+        for t in range(n_tp):
+            arrived(a_in.at[e, t], a_recv.at[e, t])
+        block = a_in[e, 0].astype(f32)
+        for t in range(1, n_tp):
+            block = block + a_in[e, t].astype(f32)
+        block = block.astype(bf16).astype(f32)
+        squares = squares + jnp.sum(block * block, axis=1, keepdims=True)
+        block = (block * moe_gain[:, e * chunk : (e + 1) * chunk]).astype(bf16)
+        gated = gated + jnp.dot(
+            block, gate_w[e * chunk : (e + 1) * chunk, :], preferred_element_type=f32
+        )
+        upped = upped + jnp.dot(
+            block, up_w[e * chunk : (e + 1) * chunk, :], preferred_element_type=f32
+        )
+    scale_two = lax.rsqrt(squares * (1.0 / d_model) + rms_epsilon)
+    gated = gated * scale_two
+    upped = upped * scale_two
+    act = (gated / (1.0 + jnp.exp(-gated)) * upped).astype(bf16)
+    for t in range(n_tp):
+        down = jnp.dot(act, down_w[:, t * part : (t + 1) * part], preferred_element_type=f32)
+        for e in range(n_ep):
+            z_out[e, t] = down[e : e + 1, :]
+    for i, j in others:
+        to, side_to = lax.rem(ep + i, n_ep), lax.rem(tp + j, n_tp)
+        index = i * n_tp + j
+        push(
+            z_out.at[to, side_to],
+            z_in.at[ep, tp],
+            (to, side_to),
+            z_send.at[index],
+            z_recv.at[ep, tp],
+        )
+    pltpu.make_async_copy(z_out.at[ep, tp], z_in.at[ep, tp], z_recv.at[ep, tp]).start()
+
+    pieces = []
+    for c in range(per_part):
+        for t in range(n_tp):
+            arrived(m_in.at[c, t], m_recv.at[c, t])
+        piece = m_in[c, 0].astype(f32)
+        for t in range(1, n_tp):
+            piece = piece + m_in[c, t].astype(f32)
+        pieces.append(piece.astype(bf16).astype(f32))
+    result = jnp.concatenate(pieces, axis=1)
+    token = lax.broadcasted_iota(jnp.int32, (tokens, 128), 0)
+    expert = lax.broadcasted_iota(jnp.int32, (tokens, 128), 1)
+    mixing = jnp.zeros((tokens, 128), f32)
+    for k in range(slots):
+        share = route_weight[:, k : k + 1].astype(f32)
+        for i in range(tokens):
+            mixing = mixing + jnp.where((token == i) & (expert == chosen[i][k]), share, 0.0)
+    for e in range(n_ep):
+        for t in range(n_tp):
+            arrived(z_in.at[e, t], z_recv.at[e, t])
+        line = z_in[e, 0]
+        for t in range(1, n_tp):
+            line = line + z_in[e, t]
+        result = result + mixing[:, e : e + 1] * line
+    mixed[...] = result.astype(bf16)
+
+    for copy in sends:
+        copy.wait_send()
+
+    @pl.when(side != tp)
+    def _():
+        own.wait_send()
+
+
+def layer(
+    hidden,
+    attn_gain,
+    query_weight,
+    head_bias,
+    key_cache,
+    value_cache,
+    lengths,
+    out_weight,
+    moe_gain,
+    route_group,
+    route_inner,
+    route_weight,
+    gate_w,
+    up_w,
+    down_w,
+):
+    n_tp = lax.axis_size("tp")
+    n_ep = lax.axis_size("ep")
+    tokens, d_model = hidden.shape
+    _, local_kv, cache_len, head_size = key_cache.shape
+    chunk, width = query_weight.shape
+    part = d_model // n_tp
+    heads = width // head_size
+    rows = tokens * heads
+    slots = route_inner.shape[1]
+    experts = gate_w.shape[0] * n_ep
+    fits = (
+        gate_w.shape[0] == 1
+        and local_kv == 1
+        and chunk % 128 == 0
+        and part % chunk == 0
+        and n_ep % 8 == 0
+        and n_ep <= 16
+        and rows % 16 == 0
+        and head_size == 128
+        and cache_len % 128 == 0
+        and tokens * n_ep <= 128
+    )
+    if not fits:
+        return body(
+            hidden,
+            attn_gain,
+            query_weight,
+            head_bias,
+            key_cache,
+            value_cache,
+            lengths,
+            out_weight,
+            moe_gain,
+            route_group,
+            route_inner,
+            route_weight,
+            gate_w,
+            up_w,
+            down_w,
+        )
+    group_size = experts // max(2, experts // 32)
+    f32, bf16 = jnp.float32, jnp.bfloat16
+    smem = pl.BlockSpec(memory_space=pltpu.SMEM)
+    hbm = pl.BlockSpec(memory_space=pl.ANY)
+    vmem = pltpu.VMEM
+    dma = pltpu.SemaphoreType.DMA
+    everyone = n_ep * n_tp
+    return pl.pallas_call(
+        functools.partial(kernel, n_ep, n_tp, group_size),
+        out_shape=jax.ShapeDtypeStruct((tokens, part), bf16),
+        in_specs=[smem] * 4 + [hbm] * 11,
+        out_specs=pl.BlockSpec(memory_space=pltpu.VMEM),
+        scratch_shapes=[
+            vmem(hidden.shape, bf16),
+            vmem((1, d_model), f32),
+            vmem(query_weight.shape, bf16),
+            vmem((tokens, cache_len, head_size), bf16),
+            vmem((tokens, cache_len, head_size), bf16),
+            vmem(out_weight.shape, bf16),
+            vmem((1, d_model), f32),
+            vmem(route_weight.shape, bf16),
+            vmem(gate_w.shape[1:], bf16),
+            vmem(up_w.shape[1:], bf16),
+            vmem(down_w.shape[1:], bf16),
+            dma((11,)),
+            vmem((n_ep, tokens, chunk), bf16),
+            vmem((1, slots * 128), jnp.int32),
+            vmem((n_ep, 1, slots * 128), jnp.int32),
+            vmem((n_ep, tokens, width), f32),
+            vmem((n_ep, tokens, width), f32),
+            vmem((rows, head_size), bf16),
+            vmem((n_ep, rows, head_size), bf16),
+            vmem((n_ep, n_ep, chunk), bf16),
+            vmem((n_ep, n_tp, n_ep, chunk), bf16),
+            vmem((n_ep, tokens, chunk), bf16),
+            vmem((part // chunk, n_tp, tokens, chunk), bf16),
+            vmem((n_ep, n_tp, 1, part), f32),
+            vmem((n_ep, n_tp, 1, part), f32),
+            dma((n_ep,)),
+            dma((n_ep,)),
+            dma((n_ep,)),
+            dma((n_ep,)),
+            dma((n_ep,)),
+            dma((n_ep,)),
+            dma((n_ep,)),
+            dma((n_ep,)),
+            dma((everyone,)),
+            dma((n_ep, n_tp)),
+            dma((n_ep,)),
+            dma((part // chunk, n_tp)),
+            dma((everyone,)),
+            dma((n_ep, n_tp)),
+            vmem((tokens * n_ep, chunk), f32),
+            vmem((slots, n_ep, 128), jnp.int32),
+            vmem((rows, head_size), f32),
+            vmem((rows, cache_len), f32),
+            vmem((rows, cache_len), f32),
+            vmem((rows * n_ep, head_size), f32),
+        ],
+        compiler_params=pltpu.CompilerParams(
+            collective_id=0, has_side_effects=True, vmem_limit_bytes=60 * 1024 * 1024
+        ),
+    )(
+        head_bias,
+        lengths,
+        route_group,
+        route_inner,
+        hidden,
+        attn_gain.reshape(1, d_model),
+        query_weight,
+        key_cache,
+        value_cache,
+        out_weight,
+        moe_gain.reshape(1, d_model),
+        route_weight,
+        gate_w,
+        up_w,
+        down_w,
+    )
+
+
 def solution(mesh):
     placed = (
         P("ep", None),
@@ -125,4 +635,4 @@
         P("ep", None, "tp"),
         P("ep", "tp", None),
     )
-    return jax.shard_map(body, mesh=mesh, in_specs=placed, out_specs=P("ep", "tp"), check_vma=False)
+    return jax.shard_map(layer, mesh=mesh, in_specs=placed, out_specs=P("ep", "tp"), check_vma=False)

time: 151 us -> 40.7 us (0.27)
  blocking collectives: 56.9 us -> 0 us
  Pallas kernels: 0 us -> 33.6 us
  other arithmetic: 27.7 us -> 0 us
  waiting for transfers between devices: 25.6 us -> 0 us
  between operations: 14.1 us -> 0.01 us
  starting transfers between devices: 12.8 us -> 0 us
  matrix products: 9.09 us -> 0 us
  local copies, waits for them, and re-layouts: 4.21 us -> 6.85 us
    unnamed x1 -> x0, blocking collectives: 37.7 us -> none
    pallas_call x0 -> x1, Pallas kernels: none -> 33.6 us  [layer(): pl.pallas_call(functools.partial(kernel, n_ep, n_tp, group_size), out_sha...]
    another operation x2 -> x0, other arithmetic: 20.5 us -> none
    reduce_scatter x1 -> x0, waiting for transfers between devices: 17.1 us -> none  [body(): lax.psum_scatter(down_rounded.astype(jnp.bfloat16), 'tp', scatter_dimensi...]
    all_to_all x2 -> x0, starting transfers between devices: 12.8 us -> none  [the longest x1 7.28 us: body(): lax.all_to_all(normed, 'ep', split_axis=1, concat_axis=0, tiled=True)]
    psum x1 -> x0, blocking collectives: 10.1 us -> none  [body(): attended = lax.psum(rounded.astype(jnp.bfloat16), 'tp').astype(jnp.float32)]
    dot_general x8 -> x0, matrix products: 9.09 us -> none  [the longest x1 2.35 us: body(): jnp.einsum('tkgp,tkpd->tkgd', weight, value_cache, preferred_element_type...]
    all_to_all x1 -> x0, blocking collectives: 9.06 us -> none  [body(): lax.all_to_all(outgoing, 'ep', split_axis=0, concat_axis=0, tiled=True)]
  transfers between devices with their start and end apart: 4 -> 0, of which waited for: 3 -> 0; matrix products, arithmetic and copies ran while one was open for 22% -> 0% of each run, Pallas kernels for 0% -> 0%
where the time goes in v1:
time: 40.7 us; the launch traced here: 40.4 us
  Pallas kernels  33.6 us (83%)
  local copies, waits for them, and re-layouts  6.85 us (17%)
    pallas_call x1, Pallas kernels, layer(): pl.pallas_call(functools.partial(kernel, n_ep, n_tp, group_size), out_sha...  33.6 us
    unnamed x11, local copies, waits for them, and re-layouts  6.85 us

profile of v1, /device:TPU:0, one launch (start us, length us, event | category | flops | bytes accessed | tf_op | source)
XLA Modules:
  0.0 40.4 jit_solution(6874326119289146982)
XLA Ops:
  0.0 0.0 copy-start.2
  0.0 0.7 %copy-done.2 = bf16[4,2]{0,1:T(2,128)(2,1)S(1)} copy-done((bf16[4,2]{0,1:T(2,128)(2,1)S(1)}, bf16[4,2]{0,1:T(2,128)(2,1)}, u32[]{:S(2)}) %copy-start.2) | copy-done | bytes 40
  0.7 0.0 copy-start.1
  0.7 0.7 %copy.17.route_weight_hbm = bf16[4,2]{1,0:T(4,128)(2,1)} copy(bf16[4,2]{0,1:T(2,128)(2,1)S(1)} %copy-done.2) | data formatting | bytes 32 | tf_op args[11]
  1.3 0.0 copy-done.1
  1.3 0.7 %copy.16.route_inner = s32[4,2]{1,0:T(4,128)} copy(s32[4,2]{0,1:T(2,128)S(1)} %copy-done.1) | data formatting | bytes 64 | tf_op args[10]
  2.0 0.0 copy-start
  2.0 2.3 %copy.18.gate_hbm = bf16[1,2048,192]{2,1,0:T(8,128)(2,1)} copy(bf16[1,2048,192]{1,2,0:T(8,128)(2,1)} %param.27) | data formatting | bytes 1572864 | tf_op args[12]
  4.3 0.0 copy-done
  4.3 1.3 %copy.19.up_hbm = bf16[1,2048,192]{2,1,0:T(8,128)(2,1)} copy(bf16[1,2048,192]{1,2,0:T(8,128)(2,1)S(1)} %copy-done) | data formatting | bytes 1572864 | tf_op args[13]
  5.6 33.6 %shard_map.145 = bf16[4,512]{1,0:T(4,128)(2,1)} custom-call(f32[16]{0:T(128)} %head_bias.1, s32[4]{0:T(128)} %lengths.1, s32[4]{0:T(128)} %route_group.1, s32[4,2]{1,0:T(4,128)} %copy.16.route_inner, bf16[4,2048]{1,0:T(4,128)(2,1)} %hidden_hbm.1, f32[1,2048]{1,0:T(1,128)} %bitcast.2, bf16[256,512]{1,0:T(8,128)(2,1)} %query_hbm.1, ...), custom_call_target="tpu_custom_call" | custom-call | tf_op jit(solution)/shard_map/pallas_call | solution.py:546
  39.2 1.3 %copy.21 = bf16[4,512]{1,0:T(4,128)(2,1)} copy(bf16[4,512]{1,0:T(4,128)(2,1)} %shard_map.145) | data formatting | bytes 8192
Async XLA Ops:
  0.0 0.7 %copy-start.2 = (bf16[4,2]{0,1:T(2,128)(2,1)S(1)}, bf16[4,2]{0,1:T(2,128)(2,1)}, u32[]{:S(2)}) copy-start(bf16[4,2]{0,1:T(2,128)(2,1)} %param.26) | copy-start | bytes 52
  0.7 0.7 %copy-start.1 = (s32[4,2]{0,1:T(2,128)S(1)}, s32[4,2]{0,1:T(2,128)}, u32[]{:S(2)}) copy-start(s32[4,2]{0,1:T(2,128)} %param.25) | copy-start | bytes 100
  2.0 2.3 %copy-start = (bf16[1,2048,192]{1,2,0:T(8,128)(2,1)S(1)}, bf16[1,2048,192]{1,2,0:T(8,128)(2,1)}, u32[]{:S(2)}) copy-start(bf16[1,2048,192]{1,2,0:T(8,128)(2,1)} %param.28) | copy-start | bytes 2359300

commit v2 on v1

--- a/solution.py
+++ b/solution.py
@@ -191,7 +191,7 @@
     rows = tokens * heads
     part = d_model // n_tp
     per_part = part // chunk
-    slots = route_inner.shape[1]
+    slots = route_inner.shape[0]
 
     loads = [
         pltpu.make_async_copy(src, dst, load_sem.at[index])
@@ -223,7 +223,7 @@
     lane = lax.broadcasted_iota(jnp.int32, (1, slots * 128), 1)
     own_route = jnp.full((1, slots * 128), -1, jnp.int32)
     chosen = [
-        [route_group[i] * group_size + route_inner[i, k] for k in range(slots)]
+        [route_group[i] * group_size + route_inner[k, i] for k in range(slots)]
         for i in range(tokens)
     ]
     for i in range(tokens):
@@ -265,6 +265,17 @@
 
     wide = hidden[...].astype(f32)
     scale = lax.rsqrt(jnp.mean(wide * wide, axis=-1, keepdims=True) + rms_epsilon)
+
+    loads[7].wait()
+    shares = route_weight[...].astype(f32)
+    token = lax.broadcasted_iota(jnp.int32, (tokens, 128), 0)
+    expert = lax.broadcasted_iota(jnp.int32, (tokens, 128), 1)
+    mixing = jnp.zeros((tokens, 128), f32)
+    for k in range(slots):
+        for i in range(tokens):
+            mixing = mixing + jnp.where(
+                (token == i) & (expert == chosen[i][k]), shares[k : k + 1, i : i + 1], 0.0
+            )
 
     loads[1].wait()
     loads[2].wait()
@@ -406,10 +417,10 @@
     def _():
         pltpu.make_async_copy(m_out.at[ep], m_in.at[place, tp], m_recv.at[place, tp]).start()
 
-    for load in loads[6:]:
+    for load in (loads[6], loads[8], loads[9], loads[10]):
         load.wait()
-    gated = jnp.zeros((n_ep, gate_w.shape[1]), f32)
-    upped = jnp.zeros((n_ep, up_w.shape[1]), f32)
+    gated = jnp.zeros((n_ep, gate_w.shape[0]), f32)
+    upped = jnp.zeros((n_ep, up_w.shape[0]), f32)
     squares = jnp.zeros((n_ep, 1), f32)
     for e in range(n_ep):
         for t in range(n_tp):
@@ -420,11 +431,17 @@
         block = block.astype(bf16).astype(f32)
         squares = squares + jnp.sum(block * block, axis=1, keepdims=True)
         block = (block * moe_gain[:, e * chunk : (e + 1) * chunk]).astype(bf16)
-        gated = gated + jnp.dot(
-            block, gate_w[e * chunk : (e + 1) * chunk, :], preferred_element_type=f32
-        )
-        upped = upped + jnp.dot(
-            block, up_w[e * chunk : (e + 1) * chunk, :], preferred_element_type=f32
+        gated = gated + lax.dot_general(
+            block,
+            gate_w[:, e * chunk : (e + 1) * chunk],
+            (((1,), (1,)), ((), ())),
+            preferred_element_type=f32,
+        )
+        upped = upped + lax.dot_general(
+            block,
+            up_w[:, e * chunk : (e + 1) * chunk],
+            (((1,), (1,)), ((), ())),
+            preferred_element_type=f32,
         )
     scale_two = lax.rsqrt(squares * (1.0 / d_model) + rms_epsilon)
     gated = gated * scale_two
@@ -455,13 +472,6 @@
             piece = piece + m_in[c, t].astype(f32)
         pieces.append(piece.astype(bf16).astype(f32))
     result = jnp.concatenate(pieces, axis=1)
-    token = lax.broadcasted_iota(jnp.int32, (tokens, 128), 0)
-    expert = lax.broadcasted_iota(jnp.int32, (tokens, 128), 1)
-    mixing = jnp.zeros((tokens, 128), f32)
-    for k in range(slots):
-        share = route_weight[:, k : k + 1].astype(f32)
-        for i in range(tokens):
-            mixing = mixing + jnp.where((token == i) & (expert == chosen[i][k]), share, 0.0)
     for e in range(n_ep):
         for t in range(n_tp):
             arrived(z_in.at[e, t], z_recv.at[e, t])
@@ -556,9 +566,9 @@
             vmem((tokens, cache_len, head_size), bf16),
             vmem(out_weight.shape, bf16),
             vmem((1, d_model), f32),
-            vmem(route_weight.shape, bf16),
-            vmem(gate_w.shape[1:], bf16),
-            vmem(up_w.shape[1:], bf16),
+            vmem((slots, tokens), bf16),
+            vmem((gate_w.shape[2], d_model), bf16),
+            vmem((up_w.shape[2], d_model), bf16),
             vmem(down_w.shape[1:], bf16),
             dma((11,)),
             vmem((n_ep, tokens, chunk), bf16),
@@ -602,7 +612,7 @@
         head_bias,
         lengths,
         route_group,
-        route_inner,
+        route_inner.T,
         hidden,
         attn_gain.reshape(1, d_model),
         query_weight,
@@ -610,9 +620,9 @@
         value_cache,
         out_weight,
         moe_gain.reshape(1, d_model),
-        route_weight,
-        gate_w,
-        up_w,
+        route_weight.T,
+        gate_w.swapaxes(1, 2),
+        up_w.swapaxes(1, 2),
         down_w,
     )
 

time: 40.7 us -> 35.1 us (0.86)
  local copies, waits for them, and re-layouts: 6.85 us -> 1.28 us
    unnamed x11 -> x1, local copies, waits for them, and re-layouts: 6.85 us -> 1.28 us
where the time goes in v2:
time: 35.1 us; the launch traced here: 34.9 us
  Pallas kernels  33.6 us (96%)
  local copies, waits for them, and re-layouts  1.28 us (4%)
    pallas_call x1, Pallas kernels, layer(): pl.pallas_call(functools.partial(kernel, n_ep, n_tp, group_size), out_sha...  33.6 us
    unnamed x1, local copies, waits for them, and re-layouts  1.28 us

profile of v2, /device:TPU:0, one launch (start us, length us, event | category | flops | bytes accessed | tf_op | source)
XLA Modules:
  0.0 34.9 jit_solution(4065994854777658146)
XLA Ops:
  0.0 33.6 %shard_map.145 = bf16[4,512]{1,0:T(4,128)(2,1)} custom-call(f32[16]{0:T(128)} %head_bias.1, s32[4]{0:T(128)} %lengths.1, s32[4]{0:T(128)} %route_group.1, s32[2,4]{1,0:T(2,128)} %bitcast.10, bf16[4,2048]{1,0:T(4,128)(2,1)} %hidden_hbm.1, f32[1,2048]{1,0:T(1,128)} %bitcast.8, bf16[256,512]{1,0:T(8,128)(2,1)} %query_hbm.1, bf16[4,1,1024,128]{3,2,1,0:T(8,128)(2,1)} %key_hbm.1, ...), custom_call_target="tpu_custom_call" | custom-call | tf_op jit(solution)/shard_map/pallas_call | solution.py:556
  33.6 1.3 %copy.17 = bf16[4,512]{1,0:T(4,128)(2,1)} copy(bf16[4,512]{1,0:T(4,128)(2,1)} %shard_map.145) | data formatting | bytes 8192

commit v3 on v2

--- a/solution.py
+++ b/solution.py
@@ -118,10 +118,10 @@
     n_ep,
     n_tp,
     group_size,
-    head_bias,
-    lengths,
-    route_group,
-    route_inner,
+    head_bias_hbm,
+    lengths_hbm,
+    route_group_hbm,
+    route_inner_hbm,
     hidden_hbm,
     attn_gain_hbm,
     query_hbm,
@@ -134,6 +134,10 @@
     up_hbm,
     down_hbm,
     mixed,
+    head_bias,
+    lengths,
+    route_group,
+    route_inner,
     hidden,
     attn_gain,
     query_w,
@@ -208,11 +212,14 @@
                 (gate_hbm.at[0], gate_w),
                 (up_hbm.at[0], up_w),
                 (down_hbm.at[0], down_w),
+                (route_group_hbm, route_group),
+                (route_inner_hbm, route_inner),
+                (lengths_hbm, lengths),
+                (head_bias_hbm, head_bias),
             )
         )
     ]
-    for load in loads:
-        load.start()
+    loads[0].start()
 
     barrier = pltpu.get_barrier_semaphore()
     others = [(i, j) for i in range(n_ep) for j in range(n_tp) if (i, j) != (0, 0)]
@@ -220,6 +227,11 @@
         peer = (lax.rem(ep + i, n_ep), lax.rem(tp + j, n_tp))
         pl.semaphore_signal(barrier, inc=1, device_id=peer, device_id_type=MESH)
 
+    for load in loads[11:13] + loads[1:11] + loads[13:]:
+        load.start()
+
+    loads[11].wait()
+    loads[12].wait()
     lane = lax.broadcasted_iota(jnp.int32, (1, slots * 128), 1)
     own_route = jnp.full((1, slots * 128), -1, jnp.int32)
     chosen = [
@@ -235,6 +247,15 @@
     loads[0].wait()
 
     sends = []
+    last = n_ep - 1
+    upper = ep >= n_ep // 2
+
+    def partner(step):
+        down_to = last - step - jnp.where(last - step <= ep, 1, 0)
+        up_to = step + jnp.where(step >= ep, 1, 0)
+        return jnp.where(upper, up_to, down_to)
+
+    partners = [partner(step) for step in range(last)]
 
     def push(src, dst, peer, send_sem, recv_sem):
         copy = pltpu.make_async_remote_copy(
@@ -254,12 +275,10 @@
     def columns(index, width):
         return pl.ds(pl.multiple_of(index * width, 128), width)
 
-    for k in range(1, n_ep):
-        to = lax.rem(ep + k, n_ep)
+    for k, to in enumerate(partners):
         push(hidden.at[:, columns(to, chunk)], x_in.at[ep], (to, tp), x_send.at[k], x_recv.at[ep])
     pltpu.make_async_copy(hidden.at[:, columns(ep, chunk)], x_in.at[ep], x_recv.at[ep]).start()
-    for k in range(1, n_ep):
-        to = lax.rem(ep + k, n_ep)
+    for k, to in enumerate(partners):
         push(r_out, r_in.at[ep], (to, tp), r_send.at[k], r_recv.at[ep])
     pltpu.make_async_copy(r_out, r_in.at[ep], r_recv.at[ep]).start()
 
@@ -285,9 +304,8 @@
     features = (x_all[...] * attn_gain[:, columns(ep, chunk)]).astype(bf16)
     query_parts = jnp.dot(features, query_w[...], preferred_element_type=f32)
     for e in range(n_ep):
-        q_out[e] = query_parts[e * tokens : (e + 1) * tokens, :]
-    for k in range(1, n_ep):
-        to = lax.rem(ep + k, n_ep)
+        q_out[e] = query_parts[e * tokens : (e + 1) * tokens, :].astype(bf16)
+    for k, to in enumerate(partners):
         push(q_out.at[to], q_in.at[ep], (to, tp), q_send.at[k], q_recv.at[ep])
     pltpu.make_async_copy(q_out.at[ep], q_in.at[ep], q_recv.at[ep]).start()
 
@@ -304,6 +322,8 @@
         picks.append(jnp.where(hit, 1.0, 0.0))
     pick = jnp.concatenate(picks, axis=0)[:, :total].astype(bf16)
 
+    loads[13].wait()
+    loads[14].wait()
     row = lax.broadcasted_iota(jnp.int32, (rows, 1), 0)
     bias = jnp.zeros((rows, 1), f32)
     length = jnp.zeros((rows, 1), jnp.int32)
@@ -319,9 +339,9 @@
 
     for e in range(n_ep):
         arrived(q_in.at[e], q_recv.at[e])
-    queries = q_in[0]
+    queries = q_in[0].astype(f32)
     for e in range(1, n_ep):
-        queries = queries + q_in[e]
+        queries = queries + q_in[e].astype(f32)
     queries = queries * scale
     for i in range(tokens):
         for h in range(heads):
@@ -368,8 +388,7 @@
             preferred_element_type=f32,
         )
     h_out[...] = head_rows[:rows, :].astype(bf16)
-    for k in range(1, n_ep):
-        to = lax.rem(ep + k, n_ep)
+    for k, to in enumerate(partners):
         push(h_out, h_in.at[ep], (to, tp), h_send.at[k], h_recv.at[ep])
     pltpu.make_async_copy(h_out, h_in.at[ep], h_recv.at[ep]).start()
 
@@ -387,23 +406,22 @@
     picked = jnp.dot(pick, summed.astype(bf16), preferred_element_type=f32)
     for e in range(n_ep):
         a_out[e] = picked[e * n_ep : (e + 1) * n_ep, :].astype(bf16)
-    for i, j in others:
-        to, side = lax.rem(ep + i, n_ep), lax.rem(tp + j, n_tp)
-        index = i * n_tp + j
+    routes = [(to, lax.rem(tp + n_tp - 1 - j, n_tp)) for to in partners for j in range(n_tp)]
+    routes += [(ep, lax.rem(tp + j, n_tp)) for j in range(1, n_tp)]
+    for index, (to, side) in enumerate(routes):
         push(a_out.at[to], a_in.at[ep, tp], (to, side), a_send.at[index], a_recv.at[ep, tp])
     pltpu.make_async_copy(a_out.at[ep], a_in.at[ep, tp], a_recv.at[ep, tp]).start()
 
     for e in range(n_ep):
         m_out[e] = summed[e * tokens : (e + 1) * tokens, :].astype(bf16)
     side, place = ep // per_part, lax.rem(ep, per_part)
-    for k in range(1, n_ep):
-        to = lax.rem(ep + k, n_ep)
+    for k, to in enumerate(partners):
         push(m_out.at[to], m_in.at[place, tp], (to, side), m_send.at[k], m_recv.at[place, tp])
 
     own = pltpu.make_async_remote_copy(
         src_ref=m_out.at[ep],
         dst_ref=m_in.at[place, tp],
-        send_sem=m_send.at[0],
+        send_sem=m_send.at[last],
         recv_sem=m_recv.at[place, tp],
         device_id=(ep, side),
         device_id_type=MESH,
@@ -450,10 +468,10 @@
     for t in range(n_tp):
         down = jnp.dot(act, down_w[:, t * part : (t + 1) * part], preferred_element_type=f32)
         for e in range(n_ep):
-            z_out[e, t] = down[e : e + 1, :]
-    for i, j in others:
-        to, side_to = lax.rem(ep + i, n_ep), lax.rem(tp + j, n_tp)
-        index = i * n_tp + j
+            z_out[e, t] = jnp.concatenate(
+                [down[e : e + 1, : part // 2], down[e : e + 1, part // 2 :]], axis=0
+            ).astype(bf16)
+    for index, (to, side_to) in enumerate(routes):
         push(
             z_out.at[to, side_to],
             z_in.at[ep, tp],
@@ -475,9 +493,10 @@
     for e in range(n_ep):
         for t in range(n_tp):
             arrived(z_in.at[e, t], z_recv.at[e, t])
-        line = z_in[e, 0]
+        line = z_in[e, 0].astype(f32)
         for t in range(1, n_tp):
-            line = line + z_in[e, t]
+            line = line + z_in[e, t].astype(f32)
+        line = jnp.concatenate([line[0:1, :], line[1:2, :]], axis=1)
         result = result + mixing[:, e : e + 1] * line
     mixed[...] = result.astype(bf16)
 
@@ -521,6 +540,7 @@
         and local_kv == 1
         and chunk % 128 == 0
         and part % chunk == 0
+        and part % 256 == 0
         and n_ep % 8 == 0
         and n_ep <= 16
         and rows % 16 == 0
@@ -548,17 +568,20 @@
         )
     group_size = experts // max(2, experts // 32)
     f32, bf16 = jnp.float32, jnp.bfloat16
-    smem = pl.BlockSpec(memory_space=pltpu.SMEM)
-    hbm = pl.BlockSpec(memory_space=pl.ANY)
+    hbm = pl.BlockSpec(memory_space=pltpu.HBM)
     vmem = pltpu.VMEM
     dma = pltpu.SemaphoreType.DMA
     everyone = n_ep * n_tp
     return pl.pallas_call(
         functools.partial(kernel, n_ep, n_tp, group_size),
-        out_shape=jax.ShapeDtypeStruct((tokens, part), bf16),
-        in_specs=[smem] * 4 + [hbm] * 11,
+        out_shape=pltpu.VMEM((tokens, part), bf16),
+        in_specs=[hbm] * 15,
         out_specs=pl.BlockSpec(memory_space=pltpu.VMEM),
         scratch_shapes=[
+            pltpu.SMEM(head_bias.shape, f32),
+            pltpu.SMEM(lengths.shape, jnp.int32),
+            pltpu.SMEM(route_group.shape, jnp.int32),
+            pltpu.SMEM((slots, tokens), jnp.int32),
             vmem(hidden.shape, bf16),
             vmem((1, d_model), f32),
             vmem(query_weight.shape, bf16),
@@ -570,20 +593,20 @@
             vmem((gate_w.shape[2], d_model), bf16),
             vmem((up_w.shape[2], d_model), bf16),
             vmem(down_w.shape[1:], bf16),
-            dma((11,)),
+            dma((15,)),
             vmem((n_ep, tokens, chunk), bf16),
             vmem((1, slots * 128), jnp.int32),
             vmem((n_ep, 1, slots * 128), jnp.int32),
-            vmem((n_ep, tokens, width), f32),
-            vmem((n_ep, tokens, width), f32),
+            vmem((n_ep, tokens, width), bf16),
+            vmem((n_ep, tokens, width), bf16),
             vmem((rows, head_size), bf16),
             vmem((n_ep, rows, head_size), bf16),
             vmem((n_ep, n_ep, chunk), bf16),
             vmem((n_ep, n_tp, n_ep, chunk), bf16),
             vmem((n_ep, tokens, chunk), bf16),
             vmem((part // chunk, n_tp, tokens, chunk), bf16),
-            vmem((n_ep, n_tp, 1, part), f32),
-            vmem((n_ep, n_tp, 1, part), f32),
+            vmem((n_ep, n_tp, 2, part // 2), bf16),
+            vmem((n_ep, n_tp, 2, part // 2), bf16),
             dma((n_ep,)),
             dma((n_ep,)),
             dma((n_ep,)),

time: 35.1 us -> 32.2 us (0.917)
  Pallas kernels: 33.6 us -> 31.5 us
  local copies, waits for them, and re-layouts: 1.28 us -> 0.6 us
    pallas_call x1, Pallas kernels: 33.6 us -> 31.5 us  [layer(): pl.pallas_call(functools.partial(kernel, n_ep, n_tp, group_size), out_sha...]
    unnamed x1, local copies, waits for them, and re-layouts: 1.28 us -> 0.6 us
where the time goes in v3:
time: 32.2 us; the launch traced here: 32.1 us
  Pallas kernels  31.5 us (98%)
  local copies, waits for them, and re-layouts  0.6 us (2%)
    pallas_call x1, Pallas kernels, layer(): pl.pallas_call(functools.partial(kernel, n_ep, n_tp, group_size), out_sha...  31.5 us

profile of v3, /device:TPU:0, one launch (start us, length us, event | category | flops | bytes accessed | tf_op | source)
XLA Modules:
  0.0 32.1 jit_solution(11361901062649824063)
XLA Ops:
  0.0 31.5 %shard_map.145 = bf16[4,512]{1,0:T(4,128)(2,1)S(1)} custom-call(f32[16]{0:T(128)} %head_bias_hbm.1, s32[4]{0:T(128)} %lengths_hbm.1, s32[4]{0:T(128)} %route_group_hbm.1, s32[2,4]{1,0:T(2,128)} %bitcast.10, bf16[4,2048]{1,0:T(4,128)(2,1)} %hidden_hbm.1, f32[1,2048]{1,0:T(1,128)} %bitcast.8, bf16[256,512]{1,0:T(8,128)(2,1)} %query_hbm.1, ...), custom_call_target="tpu_custom_call" | custom-call | tf_op jit(solution)/shard_map/pallas_call | solution.py:575
  31.5 0.6 %copy.17 = bf16[4,512]{1,0:T(4,128)(2,1)} copy(bf16[4,512]{1,0:T(4,128)(2,1)S(1)} %shard_map.145) | data formatting | bytes 8192

commit v4 on v3

--- a/solution.py
+++ b/solution.py
@@ -222,7 +222,7 @@
     loads[0].start()
 
     barrier = pltpu.get_barrier_semaphore()
-    others = [(i, j) for i in range(n_ep) for j in range(n_tp) if (i, j) != (0, 0)]
+    others = [(i, 0) for i in range(1, n_ep)] + [(0, j) for j in range(1, n_tp)]
     for i, j in others:
         peer = (lax.rem(ep + i, n_ep), lax.rem(tp + j, n_tp))
         pl.semaphore_signal(barrier, inc=1, device_id=peer, device_id_type=MESH)

time: 32.2 us -> 31.4 us (0.975)
  Pallas kernels: 31.5 us -> 30.7 us
    pallas_call x1, Pallas kernels: 31.5 us -> 30.7 us  [layer(): pl.pallas_call(functools.partial(kernel, n_ep, n_tp, group_size), out_sha...]
where the time goes in v4:
time: 31.4 us; the launch traced here: 31.3 us
  Pallas kernels  30.7 us (98%)
  local copies, waits for them, and re-layouts  0.6 us (2%)
    pallas_call x1, Pallas kernels, layer(): pl.pallas_call(functools.partial(kernel, n_ep, n_tp, group_size), out_sha...  30.7 us

profile of v4, /device:TPU:0, one launch (start us, length us, event | category | flops | bytes accessed | tf_op | source)
XLA Modules:
  0.0 31.3 jit_solution(8487522888101090562)
XLA Ops:
  0.0 30.7 %shard_map.145 = bf16[4,512]{1,0:T(4,128)(2,1)S(1)} custom-call(f32[16]{0:T(128)} %head_bias_hbm.1, s32[4]{0:T(128)} %lengths_hbm.1, s32[4]{0:T(128)} %route_group_hbm.1, s32[2,4]{1,0:T(2,128)} %bitcast.10, bf16[4,2048]{1,0:T(4,128)(2,1)} %hidden_hbm.1, f32[1,2048]{1,0:T(1,128)} %bitcast.8, bf16[256,512]{1,0:T(8,128)(2,1)} %query_hbm.1, ...), custom_call_target="tpu_custom_call" | custom-call | tf_op jit(solution)/shard_map/pallas_call | solution.py:575
  30.7 0.6 %copy.17 = bf16[4,512]{1,0:T(4,128)(2,1)} copy(bf16[4,512]{1,0:T(4,128)(2,1)S(1)} %shard_map.145) | data formatting | bytes 8192
